TPU v7x, 32 devices: a whole 2x2x4 slice. The times are simulated.
32 devices in a mesh: grp: 2 (over y), sp: 4 (over z), tp: 4 (over x, core).
Axes of the slice: x: 2, y: 2, z: 4, core: 2. Of those that a mesh axis runs over, the one named last changes fastest.
Arguments:
- latent: bfloat16 [4096, 4096], P(('grp', 'sp', 'tp')), parts along dimension 0, may hold values from -260 to 260
- context: bfloat16 [1536, 4096], P(('grp', 'sp')), parts along dimension 0, may hold values from -6 to 6
- conditioning: bfloat16 [8192], P(('grp', 'sp')), parts along dimension 0, may hold values from -6 to 6
- norm_gain: float32 [4096], replicated, may hold values from 0.1 to 1.9
- shift_weight: bfloat16 [4096, 4096], P('sp', 'tp'), may hold values from -0.09375 to 0.09375
- scale_weight: bfloat16 [4096, 4096], P('sp', 'tp'), may hold values from -0.09375 to 0.09375
- gate_weight: bfloat16 [4096, 4096], P('sp', 'tp'), may hold values from -0.09375 to 0.09375
- query_weight: bfloat16 [4096, 1024], P(None, 'tp'), may hold values from -3 to 3
- key_weight: bfloat16 [4096, 512], P(None, 'tp'), may hold values from -3 to 3
- value_weight: bfloat16 [4096, 512], P(None, 'tp'), may hold values from -0.09375 to 0.09375
- out_weight: bfloat16 [1024, 4096], P(None, 'tp'), may hold values from -1.5 to 1.5
- sink_logit: float32 [16], P('tp'), may hold values from 3 to 7
Outputs:
- mixed: bfloat16 [4096, 4096], P(('grp', 'sp', 'tp')), parts along dimension 0
There are 2 independent parts, one for each index of `grp`. A program takes and returns all parts, laid end to end along the dimension named above; an argument that names none is the same for every part. Nothing has to cross between parts.
All inputs are finite; a program needn't handle non-finite values.
Results may differ from a plain program's by a relative error of at most 0.012.
The roundings to bfloat16 on the way count: a program that leaves them out, or rounds other values in their place, can miss the bound.
Values may be sent and summed in bfloat16 or wider, within the bound.
A program may use at most 64 MiB of HBM per device.

v0:
```python
import jax
import jax.numpy as jnp
from jax import lax
from jax.sharding import PartitionSpec as P

HEADS = 16
KV_HEADS = 8
HD = 64
GRID_W = 64
WIN = 128


epsilon = 1e-06
rope_base = 10000.0
neg_large = -1e30


def with_halo(cells, sides, width):
    for axis, dim in sides:
        count = lax.axis_size(axis)
        ends = count - 1
        head = lax.slice_in_dim(cells, 0, width, axis=dim)
        tail = lax.slice_in_dim(cells, cells.shape[dim] - width, cells.shape[dim], axis=dim)
        cells = jnp.concatenate(
            [
                lax.ppermute(tail, axis, [(i, (i + 1) % count) for i in range(ends)]),
                cells,
                lax.ppermute(head, axis, [((i + 1) % count, i) for i in range(ends)]),
            ],
            axis=dim,
        )
    return cells


def row_norm(matrix, norm_gain):
    values = matrix.astype(jnp.float32)
    return (
        values * lax.rsqrt(jnp.mean(values * values, axis=-1, keepdims=True) + epsilon) * norm_gain
    )


def axial_turn(values, position):
    half_dim = values.shape[-1] // 2
    quarter = half_dim // 2
    inverse = rope_base ** (-jnp.arange(quarter, dtype=jnp.float32) / quarter)

    def turn(section, coordinate):
        angles = coordinate.astype(jnp.float32)[:, None] * inverse[None, :]
        cosine = jnp.cos(angles)[:, None, :]
        sine_part = jnp.sin(angles)[:, None, :]
        leading = section[..., :quarter]
        trailing = section[..., quarter:]
        return jnp.concatenate(
            [leading * cosine - trailing * sine_part, leading * sine_part + trailing * cosine],
            axis=-1,
        )

    return jnp.concatenate(
        [
            turn(values[..., :half_dim], position // GRID_W),
            turn(values[..., half_dim:], position % GRID_W),
        ],
        axis=-1,
    )


def context_pairs(context_rows, norm_gain, key_weight, value_weight):
    prepared = row_norm(context_rows, norm_gain).astype(jnp.bfloat16)
    return jnp.concatenate(
        [
            jnp.dot(prepared, key_weight, preferred_element_type=jnp.float32),
            jnp.dot(prepared, value_weight, preferred_element_type=jnp.float32),
        ],
        axis=1,
    ).astype(jnp.bfloat16)


def local(
    latent,
    context,
    conditioning,
    norm_gain,
    shift_weight,
    scale_weight,
    gate_weight,
    query_weight,
    key_weight,
    value_weight,
    out_weight,
    sink_logit,
):
    lifted = jax.nn.silu(conditioning.astype(jnp.float32)).astype(jnp.bfloat16)[None, :]
    shift_part = jnp.dot(lifted, shift_weight, preferred_element_type=jnp.float32)[0]
    scale_part = jnp.dot(lifted, scale_weight, preferred_element_type=jnp.float32)[0]
    gate_part = jnp.dot(lifted, gate_weight, preferred_element_type=jnp.float32)[0]
    summed = lax.psum((shift_part, scale_part, gate_part), "sp")
    shift_vec, scale_vec, gate_vec = (
        lax.all_gather(summed[0], "tp", axis=0, tiled=True),
        lax.all_gather(summed[1], "tp", axis=0, tiled=True),
        lax.all_gather(summed[2], "tp", axis=0, tiled=True),
    )
    normed = (row_norm(latent, norm_gain) * (1.0 + scale_vec) + shift_vec).astype(jnp.bfloat16)
    segment = lax.all_gather(normed, "tp", axis=0, tiled=True)
    projected = jnp.concatenate(
        [
            jnp.dot(segment, query_weight, preferred_element_type=jnp.float32),
            jnp.dot(segment, key_weight, preferred_element_type=jnp.float32),
            jnp.dot(segment, value_weight, preferred_element_type=jnp.float32),
        ],
        axis=1,
    )
    row_count = projected.shape[0]
    query_width = query_weight.shape[1]
    key_width = key_weight.shape[1]
    query_heads = query_width // HD
    pair_heads = key_width // HD
    group_size = HEADS // KV_HEADS
    row_offset = lax.axis_index("sp") * row_count
    position = row_offset + jnp.arange(row_count, dtype=jnp.int32)
    queries = axial_turn(
        projected[:, :query_width].reshape(row_count, query_heads, HD), position
    ).astype(jnp.bfloat16)
    latent_keys = axial_turn(
        projected[:, query_width : query_width + key_width].reshape(row_count, pair_heads, HD),
        position,
    ).astype(jnp.bfloat16)
    latent_values = projected[:, query_width + key_width :].astype(jnp.bfloat16)
    key_value = jnp.concatenate([latent_keys.reshape(row_count, key_width), latent_values], axis=1)
    widened = with_halo(key_value, (("sp", 0),), WIN)
    context_all = lax.all_gather(
        context_pairs(context, norm_gain, key_weight, value_weight), "sp", axis=0, tiled=True
    )
    block_count = row_count // WIN
    context_count = context_all.shape[0]
    query_blocks = queries.reshape(block_count, WIN, pair_heads, group_size, HD)
    band_blocks = widened.reshape(block_count + 2, WIN, 2 * key_width)
    band_rows = jnp.concatenate(
        [band_blocks[:block_count], band_blocks[1 : block_count + 1], band_blocks[2:]], axis=1
    )
    band_keys = band_rows[..., :key_width].reshape(block_count, 3 * WIN, pair_heads, HD)
    band_values = band_rows[..., key_width:].reshape(block_count, 3 * WIN, pair_heads, HD)
    context_keys = context_all[:, :key_width].reshape(context_count, pair_heads, HD)
    context_values = context_all[:, key_width:].reshape(context_count, pair_heads, HD)
    factor = HD ** (-0.5)
    local_scores = (
        jnp.einsum("nqhgd,nkhd->nhgqk", query_blocks, band_keys, preferred_element_type=jnp.float32)
        * factor
    )
    query_pos = position.reshape(block_count, WIN)
    key_pos = (
        row_offset
        - WIN
        + jnp.arange(block_count, dtype=jnp.int32)[:, None] * WIN
        + jnp.arange(3 * WIN, dtype=jnp.int32)[None, :]
    )
    seq_total = row_count * lax.axis_size("sp")
    allowed = (
        (jnp.abs(key_pos[:, None, :] - query_pos[:, :, None]) <= WIN)
        & (key_pos[:, None, :] >= 0)
        & (key_pos[:, None, :] < seq_total)
    )
    local_scores = jnp.where(allowed[:, None, None], local_scores, neg_large)
    context_scores = (
        jnp.einsum(
            "nqhgd,thd->nhgqt", query_blocks, context_keys, preferred_element_type=jnp.float32
        )
        * factor
    )
    sink_values = sink_logit.reshape(pair_heads, group_size)[None, :, :, None, None]
    highest = jnp.maximum(
        jnp.maximum(
            jnp.max(local_scores, axis=-1, keepdims=True),
            jnp.max(context_scores, axis=-1, keepdims=True),
        ),
        sink_values,
    )
    local_exp = jnp.exp(local_scores - highest)
    context_exp = jnp.exp(context_scores - highest)
    denominator = (
        jnp.sum(local_exp, axis=-1, keepdims=True)
        + jnp.sum(context_exp, axis=-1, keepdims=True)
        + jnp.exp(sink_values - highest)
    )
    local_weights = (local_exp / denominator).astype(jnp.bfloat16)
    context_weights = (context_exp / denominator).astype(jnp.bfloat16)
    attended = jnp.einsum(
        "nhgqk,nkhd->nqhgd", local_weights, band_values, preferred_element_type=jnp.float32
    ) + jnp.einsum(
        "nhgqt,thd->nqhgd", context_weights, context_values, preferred_element_type=jnp.float32
    )
    attended = attended.reshape(row_count, query_width).astype(jnp.bfloat16)
    columns_part = jnp.dot(
        lax.all_gather(attended, "tp", axis=1, tiled=True),
        out_weight,
        preferred_element_type=jnp.float32,
    ).astype(jnp.bfloat16)
    blended = lax.all_to_all(columns_part, "tp", split_axis=0, concat_axis=1, tiled=True)
    return (latent.astype(jnp.float32) + gate_vec * blended.astype(jnp.float32)).astype(
        jnp.bfloat16
    )


def solution(mesh):
    in_specs = (
        P(("grp", "sp", "tp"), None),
        P(("grp", "sp"), None),
        P(("grp", "sp")),
        P(),
        P("sp", "tp"),
        P("sp", "tp"),
        P("sp", "tp"),
        P(None, "tp"),
        P(None, "tp"),
        P(None, "tp"),
        P(None, "tp"),
        P("tp"),
    )
    out_specs = P(("grp", "sp", "tp"), None)
    return jax.shard_map(local, mesh=mesh, in_specs=in_specs, out_specs=out_specs, check_vma=False)
```

profile of v0, /device:TPU:0, one launch (start us, length us, event | category | flops | bytes accessed | tf_op | source)
XLA Modules:
  0.0 175.9 jit_solution(4431340669027265532)
XLA Ops:
  6.5 0.8 fusion.41
  7.4 2.1 %fusion.53 = f32[1,1024]{1,0:T(1,128)S(1)} fusion(bf16[1024,1]{0,1:T(2,128)(2,1)S(1)} %reshape.312, bf16[1024,1024]{1,0:T(8,128)(2,1)} %param.16), kind=kOutput, calls=%fused_computation.111 | convolution fusion | flops 2097152 | bytes 2103296 | tf_op jit(solution)/shard_map/dot_general | solution.py:93
  9.5 2.0 %fusion.52 = f32[1,1024]{1,0:T(1,128)S(1)} fusion(bf16[1024,1]{0,1:T(2,128)(2,1)S(1)} %reshape.312, bf16[1024,1024]{1,0:T(8,128)(2,1)} %param.17), kind=kOutput, calls=%fused_computation.110 | convolution fusion | flops 2097152 | bytes 2103296 | tf_op jit(solution)/shard_map/dot_general | solution.py:94
  11.9 20.5 %all-reduce = (f32[1024]{0:T(1024)S(1)}, f32[1024]{0:T(1024)S(1)}, f32[1024]{0:T(1024)S(1)}) all-reduce(f32[1024]{0:T(1024)S(1)} %bitcast.115, f32[1024]{0:T(1024)S(1)} %bitcast.116, f32[1024]{0:T(1024)S(1)} %bitcast.117), channel_id=1, replica_groups=mesh['grp'=2,'sp'=4,'tp'=4] {'sp'}, use_global_device_ids=true, to_apply=%region_3.4 | all-reduce | flops 3072 | bytes 24576 | tf_op jit(solution)/shard_map/psum | solution.py:96
  32.4 5.2 %all_gather.20 = f32[4096]{0:T(1024)S(1)} all-gather(f32[1024]{0:T(1024)S(1)} %get-tuple-element.5), channel_id=1, replica_groups=mesh['grp'=2,'sp'=4,'tp'=4] {'tp'}, dimensions={0}, use_global_device_ids=true | all-gather | bytes 20480 | tf_op jit(solution)/shard_map/all_gather | solution.py:98
  37.6 5.2 %all_gather.19 = f32[4096]{0:T(1024)S(1)} all-gather(f32[1024]{0:T(1024)S(1)} %get-tuple-element.6), channel_id=1, replica_groups=mesh['grp'=2,'sp'=4,'tp'=4] {'tp'}, dimensions={0}, use_global_device_ids=true | all-gather | bytes 20480 | tf_op jit(solution)/shard_map/all_gather | solution.py:99
  43.1 1.4 fusion.13
  44.6 2.0 %fusion.2 = f32[192]{0:T(256)S(1)} fusion(bf16[192,4096]{1,0:T(8,128)(2,1)} %param.13), kind=kLoop, calls=%fused_computation.7 | loop fusion | flops 2359104 | bytes 1573632 | tf_op jit(solution)/shard_map/reduce_sum | solution.py:38
  46.5 2.4 %convolution_convert_fusion.2 = bf16[192,128]{1,0:T(8,128)(2,1)S(1)} fusion(bf16[4096,128]{1,0:T(8,128)(2,1)} %param.21, bf16[192,4096]{1,0:T(8,128)(2,1)} %param.13, f32[4096]{0:T(1024)S(1)} %copy-done.16, f32[192]{0:T(256)S(1)} %add_rsqrt_fusion), kind=kOutput, calls=%fused_computation.34 | convolution fusion | flops 204496896 | bytes 2687744 | tf_op jit(solution)/shard_map/dot_general | solution.py:72
  48.9 0.7 convolution_convert_fusion.3
  49.7 15.2 %all_gather.22 = bf16[768,256]{1,0:T(8,128)(2,1)S(1)} all-gather(bf16[192,256]{1,0:T(8,128)(2,1)S(1)} %pad_maximum_fusion.6), channel_id=1, replica_groups=mesh['grp'=2,'sp'=4,'tp'=4] {'sp'}, dimensions={0}, use_global_device_ids=true | all-gather | bytes 491520 | tf_op jit(solution)/shard_map/all_gather | solution.py:130
  64.9 0.8 copy.78
  65.8 0.8 copy.88
  67.1 0.9 fusion.27
  68.1 9.3 %all-gather.3.cloned.1.call-done = bf16[512,4096]{1,0:T(8,128)(2,1)} async-done(((bf16[128,4096]{1,0:T(8,128)(2,1)}), bf16[512,4096]{1,0:T(8,128)(2,1)}) %all-gather.3.cloned.1.call-update) | async-done | bytes 4194320 | tf_op jit(solution)/shard_map/all_gather | solution.py:103
  77.3 4.1 %fusion.54 = f32[512,128]{0,1:T(8,128)S(1)} fusion(bf16[512,4096]{1,0:T(8,128)(2,1)} %all-gather.3.cloned.1.call-done, bf16[4096,128]{1,0:T(8,128)(2,1)} %param.20), kind=kOutput, calls=%fused_computation.112 | convolution fusion | flops 536870912 | bytes 5505024 | tf_op jit(solution)/shard_map/dot_general | solution.py:107
  81.6 1.5 convolution_convert_fusion.1
  83.2 0.7 fusion.33
  83.8 1.3 collective-permute-start.1
  85.1 5.3 %collective-permute-start = (bf16[128,256]{0,1:T(8,128)(2,1)}, bf16[128,256]{0,1:T(8,128)(2,1)}, u32[]{:S(2)}, u32[]{:S(2)}) collective-permute-start(bf16[128,256]{0,1:T(8,128)(2,1)} %get-tuple-element.26), channel_id=1, source_target_pairs={{0,4},{4,8},{8,12},{1,5},{5,9},{9,13},{2,6},{6,10},{10,14},{3,7},{... | collective-permute-start | bytes 196616 | tf_op jit(solution)/shard_map/ppermute | solution.py:26
  90.4 1.3 fusion.55
  91.8 0.8 add_convert_fusion
  92.5 0.9 concatenate.39
  94.0 0.9 concatenate.40
  94.9 1.5 concatenate.41
  96.4 1.5 concatenate.42
  98.5 1.5 copy_dynamic-update-slice_fusion.1
  100.0 1.5 copy_dynamic-update-slice_fusion
  101.5 4.8 %bitcast_reduce_fusion = (f32[4,2,2,128]{3,2,0,1:T(2,128)S(1)}, f32[2,768,4,128,2]{3,1,4,2,0:T(8,128)}) fusion(bf16[768,2,64,1,1]{0,2,4,3,1:T(8,128)(2,1)} %bitcast.111, bf16[4,128,2,2,64]{1,4,3,2,0:T(8,128)(2,1)} %copy_dynamic-update-slice_fusion), kind=kOutput, calls=%fused_computation.1 | convolution fusion | flops 204470272 | bytes 6758400 | tf_op jit(solution)/shard_map/nqhgd,thd->nhgqt/dot_general | solution.py:164
  106.3 1.8 %pad_maximum_fusion.1 = (bf16[512,256]{0,1:T(8,128)(2,1)}, bf16[512,256]{0,1:T(8,128)(2,1)}, bf16[512,256]{0,1:T(8,128)(2,1)}) fusion(bf16[128,256]{0,1:T(8,128)(2,1)} %collective-permute-done.1, bf16[512,128]{0,1:T(8,128)(2,1)S(1)} %convolution_convert_fusion.1, bf16[512,128]{0,1:T(8,128)(2,1)S(1)} %bitcast.108, bf16[128,256]{0,1:T(8,128)(2,1)} %collective-permute-done), kind=kLoop, calls=%fused_computation.45 | loop fusion | flops 2097152 | bytes 1179648 | tf_op jit(solution)/shard_map/concatenate | solution.py:24
  108.1 1.7 slice.78
  109.8 1.7 constant_dynamic-update-slice_fusion.2
  111.6 1.7 slice.79
  113.3 1.7 slice.82
  115.0 1.8 %constant_dynamic-update-slice_fusion.1 = bf16[4,384,256]{1,0,2:T(4,128)(2,1)} fusion(bf16[4,384,256]{1,0,2:T(4,128)(2,1)} %constant_dynamic-update-slice_fusion.2, bf16[4,128,256]{1,0,2:T(4,128)(2,1)} %slice.79), kind=kLoop, calls=%fused_computation.72 | loop fusion | bytes 524288
  116.8 1.7 constant_dynamic-update-slice_fusion
  118.5 1.5 fusion.49
  121.6 1.1 fusion.1
  122.6 0.7 fusion.7
  123.5 0.9 fusion.22
  124.4 1.4 fusion.23
  126.1 0.7 copy.127
  126.8 16.1 %all-gather.5.cloned.1.call-done = bf16[512,1024]{0,1:T(8,128)(2,1)} async-done(((bf16[512,256]{0,1:T(8,128)(2,1)}), bf16[512,1024]{0,1:T(8,128)(2,1)}) %all-gather.5.cloned.1.call-update) | async-done | bytes 1048592 | tf_op jit(solution)/shard_map/all_gather | solution.py:193
  142.9 3.5 %convolution_convert_fusion = bf16[512,1024]{1,0:T(8,128)(2,1)} fusion(bf16[512,1024]{0,1:T(8,128)(2,1)} %all-gather.5.cloned.1.call-done, bf16[1024,1024]{1,0:T(8,128)(2,1)S(1)} %copy-done), kind=kOutput, calls=%fused_computation.28 | convolution fusion | flops 1074266112 | bytes 4194304 | tf_op jit(solution)/shard_map/dot_general | solution.py:192
  146.4 4.2 %all-to-all-start = ((bf16[4,128,1024]{2,1,0:T(8,128)(2,1)}), bf16[4,128,1024]{2,1,0:T(8,128)(2,1)}, u32[]{:S(2)}, u32[]{:S(2)}) async-start(bf16[4,128,1024]{2,1,0:T(8,128)(2,1)} %bitcast.104), calls=%async_computation | async-start | bytes 2097152 | tf_op jit(solution)/shard_map/all_to_all | solution.py:197
  150.7 15.4 %all_gather.18 = f32[4096]{0:T(1024)S(1)} all-gather(f32[1024]{0:T(1024)S(1)} %get-tuple-element.7), channel_id=1, replica_groups=mesh['grp'=2,'sp'=4,'tp'=4] {'tp'}, dimensions={0}, use_global_device_ids=true | all-gather | bytes 20480 | tf_op jit(solution)/shard_map/all_gather | solution.py:100
  166.1 1.5 convert_bitcast_fusion
  167.8 1.3 fusion.14
  (76 shorter events, 4.9 us)
Async XLA Ops:
  6.5 136.4 %copy-start = (bf16[1024,1024]{1,0:T(8,128)(2,1)S(1)}, bf16[1024,1024]{1,0:T(8,128)(2,1)}, u32[]{:S(2)}) copy-start(bf16[1024,1024]{1,0:T(8,128)(2,1)} %param.22) | copy-start | bytes 6291460
  6.5 70.8 %all-gather.3.cloned.1.call-start = ((), (), s32[]{:S(2)}) async-start(), calls=%async_computation.1 | async-start | bytes 5242880 | tf_op jit(solution)/shard_map/all_gather | solution.py:103
  6.5 5.0 %copy-start.4 = (bf16[1024,1024]{1,0:T(8,128)(2,1)S(1)}, bf16[1024,1024]{1,0:T(8,128)(2,1)}, u32[]{:S(2)}) copy-start(bf16[1024,1024]{1,0:T(8,128)(2,1)} %param.18) | copy-start | bytes 6291460
  7.4 35.4 %copy-start.3 = (bf16[128,4096]{1,0:T(8,128)(2,1)S(1)}, bf16[128,4096]{1,0:T(8,128)(2,1)}, u32[]{:S(2)}) copy-start(bf16[128,4096]{1,0:T(8,128)(2,1)} %param.12) | copy-start | bytes 3145732
  9.5 33.5 %copy-start.16 = (f32[4096]{0:T(1024)S(1)}, f32[4096]{0:T(1024)}, u32[]{:S(2)}) copy-start(f32[4096]{0:T(1024)} %param.15) | copy-start | bytes 49156
  44.5 98.4 %all-gather.5.cloned.1.call-start = ((), (), s32[]{:S(2)}) async-start(), calls=%async_computation.2 | async-start | bytes 1310720 | tf_op jit(solution)/shard_map/all_gather | solution.py:193
  44.6 4.3 %copy-start.5 = (bf16[192,4096]{1,0:T(8,128)(2,1)S(1)}, bf16[192,4096]{1,0:T(8,128)(2,1)}, u32[]{:S(2)}) copy-start(bf16[192,4096]{1,0:T(8,128)(2,1)} %param.13) | copy-start | bytes 4718596
  44.6 4.3 %copy-start.10 = (bf16[4096,128]{1,0:T(8,128)(2,1)S(1)}, bf16[4096,128]{1,0:T(8,128)(2,1)}, u32[]{:S(2)}) copy-start(bf16[4096,128]{1,0:T(8,128)(2,1)} %param.20) | copy-start | bytes 3145732
  48.9 16.8 %copy-start.18 = (f32[4]{0:T(128)S(1)}, f32[4]{0:T(128)}, u32[]{:S(2)}) copy-start(f32[4]{0:T(128)} %param.23) | copy-start | bytes 52
  67.1 14.4 %copy-start.11 = (f32[512,16]{0,1:T(8,128)}, f32[512,16]{0,1:T(8,128)S(1)}, u32[]{:S(2)}) copy-start(f32[512,16]{0,1:T(8,128)S(1)} %get-tuple-element.35) | copy-start | bytes 98308
  67.1 14.4 %copy-start.13 = (f32[512,16]{0,1:T(8,128)}, f32[512,16]{0,1:T(8,128)S(1)}, u32[]{:S(2)}) copy-start(f32[512,16]{0,1:T(8,128)S(1)} %get-tuple-element.36) | copy-start | bytes 98308
  77.3 4.2 %copy-start.1 = (bf16[512,4096]{1,0:T(8,128)(2,1)S(1)}, bf16[512,4096]{1,0:T(8,128)(2,1)}, u32[]{:S(2)}) copy-start(bf16[512,4096]{1,0:T(8,128)(2,1)} %all-gather.3.cloned.1.call-done) | copy-start | bytes 12582916
  77.3 4.3 %copy-start.9 = (bf16[4096,128]{1,0:T(8,128)(2,1)S(1)}, bf16[4096,128]{1,0:T(8,128)(2,1)}, u32[]{:S(2)}) copy-start(bf16[4096,128]{1,0:T(8,128)(2,1)} %param.21) | copy-start | bytes 3145732
  81.6 1.6 copy-start.7
  81.6 8.8 %copy-start.17 = (bf16[4096,256]{1,0:T(8,128)(2,1)S(1)}, bf16[4096,256]{1,0:T(8,128)(2,1)}, u32[]{:S(2)}) copy-start(bf16[4096,256]{1,0:T(8,128)(2,1)} %param.19) | copy-start | bytes 6291460
  83.8 22.5 %collective-permute-start.1 = (bf16[128,256]{0,1:T(8,128)(2,1)}, bf16[128,256]{0,1:T(8,128)(2,1)}, u32[]{:S(2)}, u32[]{:S(2)}) collective-permute-start(bf16[128,256]{0,1:T(8,128)(2,1)} %get-tuple-element.25), channel_id=1, source_target_pairs={{4,0},{8,4},{12,8},{5,1},{9,5},{13,9},{6,2},{10,6},{14,10},{7,3},{... | collective-permute-start | bytes 196616 | tf_op jit(solution)/shard_map/ppermute | solution.py:28
  85.1 6.6 %copy-start.12 = (f32[512,16]{0,1:T(8,128)S(1)}, f32[512,16]{0,1:T(8,128)}, u32[]{:S(2)}) copy-start(f32[512,16]{0,1:T(8,128)} %copy-done.11) | copy-start | bytes 98308
  85.1 6.6 %copy-start.14 = (f32[512,16]{0,1:T(8,128)S(1)}, f32[512,16]{0,1:T(8,128)}, u32[]{:S(2)}) copy-start(f32[512,16]{0,1:T(8,128)} %copy-done.13) | copy-start | bytes 98308
  85.1 21.1 %collective-permute-start = (bf16[128,256]{0,1:T(8,128)(2,1)}, bf16[128,256]{0,1:T(8,128)(2,1)}, u32[]{:S(2)}, u32[]{:S(2)}) collective-permute-start(bf16[128,256]{0,1:T(8,128)(2,1)} %get-tuple-element.26), channel_id=1, source_target_pairs={{0,4},{4,8},{8,12},{1,5},{5,9},{9,13},{2,6},{6,10},{10,14},{3,7},{... | collective-permute-start | bytes 196616 | tf_op jit(solution)/shard_map/ppermute | solution.py:26
  101.5 4.8 %copy-start.8 = (bf16[512,2,64]{0,2,1:T(8,128)(2,1)S(1)}, bf16[512,2,64]{0,2,1:T(8,128)(2,1)}, u32[]{:S(2)}) copy-start(bf16[512,2,64]{0,2,1:T(8,128)(2,1)} %copy-done.7) | copy-start | bytes 393220
  115.0 5.1 %copy-start.6 = (bf16[4,128,2,2,64]{1,4,3,2,0:T(8,128)(2,1)S(1)}, bf16[4,128,2,2,64]{1,4,3,2,0:T(8,128)(2,1)}, u32[]{:S(2)}) copy-start(bf16[4,128,2,2,64]{1,4,3,2,0:T(8,128)(2,1)} %copy_dynamic-update-slice_fusion) | copy-start | bytes 786436
  118.5 3.0 %copy-start.2 = (f32[2,768,4,128,2]{3,1,4,2,0:T(8,128)S(1)}, f32[2,768,4,128,2]{3,1,4,2,0:T(8,128)}, u32[]{:S(2)}) copy-start(f32[2,768,4,128,2]{3,1,4,2,0:T(8,128)} %get-tuple-element.38) | copy-start | bytes 18874372
  123.5 1.0 copy-start.15
  146.4 19.7 %all-to-all-start = ((bf16[4,128,1024]{2,1,0:T(8,128)(2,1)}), bf16[4,128,1024]{2,1,0:T(8,128)(2,1)}, u32[]{:S(2)}, u32[]{:S(2)}) async-start(bf16[4,128,1024]{2,1,0:T(8,128)(2,1)} %bitcast.104), calls=%async_computation | async-start | bytes 2097152 | tf_op jit(solution)/shard_map/all_to_all | solution.py:197
Sparse Core Ops, SparseCore 0:
  44.6 32.6 all-gather.2
  127.0 15.9 all-gather.4
where the time goes:
time: 177 us; the launch traced here: 176 us
  blocking collectives  61.4 us (35%)
  matrix products  25.8 us (15%)
  waiting for transfers between devices  25.4 us (14%)
  local copies, waits for them, and re-layouts  24.7 us (14%)
  other arithmetic  13.9 us (8%)
  between operations  13.8 us (8%)
  starting transfers between devices  10.9 us (6%)
    psum x1, blocking collectives, local(): summed = lax.psum((shift_part, scale_part, gate_part), 'sp')  20.5 us
    all_gather x1, waiting for transfers between devices, local(): lax.all_gather(attended, 'tp', axis=1, tiled=True)  16.1 us
    all_gather x1, blocking collectives, local(): lax.all_gather(summed[2], 'tp', axis=0, tiled=True)  15.4 us
    all_gather x1, blocking collectives, local(): lax.all_gather(context_pairs(context, norm_gain, key_weight, value_weight...  15.2 us
    all_gather x1, waiting for transfers between devices, local(): segment = lax.all_gather(normed, 'tp', axis=0, tiled=True)  9.26 us
    unnamed x44, local copies, waits for them, and re-layouts  7.79 us
    concatenate x5, local copies, waits for them, and re-layouts, axial_turn(): jnp.concatenate([turn(values[..., :half_dim], position // GRID_W), turn(v...  6.19 us
    ppermute x1, starting transfers between devices, with_halo(): lax.ppermute(tail, axis, [(i, (i + 1) % count) for i in range(ends)])  5.3 us
  transfers between devices with their start and end apart: 5, of which 2 were waited for; matrix products, arithmetic and copies ran while one was open for 14% of the time, Pallas kernels for 0%

commit v1 on v0

--- a/solution.py
+++ b/solution.py
@@ -1,6 +1,10 @@
+import functools
+
 import jax
 import jax.numpy as jnp
 from jax import lax
+from jax.experimental import pallas as pl
+from jax.experimental.pallas import tpu as pltpu
 from jax.sharding import PartitionSpec as P
 
 HEADS = 16
@@ -75,7 +79,7 @@
     ).astype(jnp.bfloat16)
 
 
-def local(
+def local_plain(
     latent,
     context,
     conditioning,
@@ -200,6 +204,652 @@
     )
 
 
+PIECES = 4
+NORM_ROWS = 16
+
+
+def remote(src, dst, send, recv, axis, peer):
+    return pltpu.make_async_remote_copy(
+        src_ref=src,
+        dst_ref=dst,
+        send_sem=send,
+        recv_sem=recv,
+        device_id={axis: peer},
+        device_id_type=pl.DeviceIdType.MESH,
+    )
+
+
+def fused_kernel(
+    tp,
+    sp,
+    latent,
+    context,
+    conditioning,
+    norm_gain,
+    shift_weight,
+    scale_weight,
+    gate_weight,
+    query_weight,
+    key_weight,
+    value_weight,
+    out_weight,
+    sink,
+    blended,
+    gate_out,
+    cond_v,
+    gain_v,
+    mod_w,
+    wq,
+    wk,
+    wv,
+    wo,
+    ctx_v,
+    rows_all,
+    normed,
+    mod_part,
+    mod_all,
+    factor_v,
+    shift_v,
+    gate_v,
+    turn_cos,
+    turn_sin,
+    queries,
+    key_value,
+    ctx_kv,
+    att_all,
+    out_cols,
+    load_sem,
+    pair_send,
+    pair_recv,
+    far_send,
+    far_recv,
+    fwd_send,
+    fwd_recv,
+    modsp_send,
+    modsp_recv,
+    modtp_send,
+    modtp_recv,
+    ctx_send,
+    ctx_recv,
+    halo_send,
+    halo_recv,
+    apair_send,
+    apair_recv,
+    afar_send,
+    afar_recv,
+    afwd_send,
+    afwd_recv,
+    out_send,
+    out_recv,
+):
+    t = lax.axis_index("tp")
+    s = lax.axis_index("sp")
+    chips = tp // 2
+    core = lax.rem(t, 2)
+    chip = t // 2
+    pair = chip * 2 + (1 - core)
+    rows, width = latent.shape
+    ctx_rows = context.shape[0]
+    mod_cols = shift_weight.shape[1]
+    query_width = query_weight.shape[1]
+    key_width = key_weight.shape[1]
+    heads = query_width // HD
+    group = heads // (key_width // HD)
+    total = tp * rows
+    out_width = out_weight.shape[1]
+    piece = rows // PIECES
+    f32, bf16 = jnp.float32, jnp.bfloat16
+
+    def chip_at(j):
+        return lax.rem(chip + j, chips)
+
+    def chip_from(j):
+        return lax.rem(chip + chips - j, chips)
+
+    loads = [
+        (conditioning, cond_v),
+        (shift_weight, mod_w.at[0]),
+        (scale_weight, mod_w.at[1]),
+        (gate_weight, mod_w.at[2]),
+        (norm_gain, gain_v),
+        (context, ctx_v),
+        (key_weight, wk),
+        (value_weight, wv),
+        (latent, rows_all.at[t]),
+        (query_weight, wq),
+        (out_weight, wo),
+    ]
+    loads = [pltpu.make_async_copy(a, b, load_sem.at[i]) for i, (a, b) in enumerate(loads)]
+    for load in loads:
+        load.start()
+
+    barrier = pltpu.get_barrier_semaphore()
+    for k in range(1, tp):
+        pl.semaphore_signal(
+            barrier, inc=1, device_id={"tp": lax.rem(t + k, tp)}, device_id_type=pl.DeviceIdType.MESH
+        )
+    for k in range(1, sp):
+        pl.semaphore_signal(
+            barrier, inc=1, device_id={"sp": lax.rem(s + k, sp)}, device_id_type=pl.DeviceIdType.MESH
+        )
+    pl.semaphore_wait(barrier, tp - 1 + sp - 1)
+
+    far = {}
+    for c in range(PIECES):
+        part = pl.ds(c * piece, piece)
+        for j in range(1, chips):
+            i = (j - 1) * PIECES + c
+            far[j, c] = remote(
+                latent.at[part],
+                rows_all.at[t, part],
+                far_send.at[i],
+                far_recv.at[i],
+                "tp",
+                chip_at(j) * 2 + core,
+            )
+            far[j, c].start()
+    near = remote(latent, rows_all.at[t], pair_send.at[0], pair_recv.at[0], "tp", pair)
+    near.start()
+
+    for i in range(4):
+        loads[i].wait()
+    cond = cond_v[...].astype(f32)
+    lifted = jnp.broadcast_to(cond / (1.0 + jnp.exp(-cond)), (16, cond.shape[1])).astype(bf16)
+    for i in range(3):
+        mod_part[s, :, i * mod_cols : (i + 1) * mod_cols] = jnp.dot(
+            lifted, mod_w[i], preferred_element_type=f32
+        )[0:1]
+    mods = []
+    for k in range(1, sp):
+        copy = remote(
+            mod_part.at[s],
+            mod_part.at[s],
+            modsp_send.at[k - 1],
+            modsp_recv.at[k - 1],
+            "sp",
+            lax.rem(s + k, sp),
+        )
+        copy.start()
+        mods.append(copy)
+
+    for i in range(4, 8):
+        loads[i].wait()
+
+    def norm_context(g, carry):
+        part = pl.ds(pl.multiple_of(g * NORM_ROWS, NORM_ROWS), NORM_ROWS)
+        values = ctx_v[part].astype(f32)
+        scale = lax.rsqrt(jnp.mean(values * values, axis=-1, keepdims=True) + epsilon)
+        ctx_v[part] = (values * scale * gain_v[...]).astype(bf16)
+        return carry
+
+    lax.fori_loop(0, ctx_rows // NORM_ROWS, norm_context, 0)
+    ctx_kv[s, :, :key_width] = jnp.dot(ctx_v[...], wk[...], preferred_element_type=f32).astype(bf16)
+    ctx_kv[s, :, key_width:] = jnp.dot(ctx_v[...], wv[...], preferred_element_type=f32).astype(bf16)
+    ctxs = []
+    for k in range(1, sp):
+        copy = remote(
+            ctx_kv.at[s],
+            ctx_kv.at[s],
+            ctx_send.at[k - 1],
+            ctx_recv.at[k - 1],
+            "sp",
+            lax.rem(s + k, sp),
+        )
+        copy.start()
+        ctxs.append(copy)
+
+    for copy in mods:
+        copy.wait()
+    summed = mod_part[0]
+    for k in range(1, sp):
+        summed = summed + mod_part[k]
+    mod_all[t] = summed
+    mods = []
+    for k in range(1, tp):
+        copy = remote(
+            mod_all.at[t],
+            mod_all.at[t],
+            modtp_send.at[k - 1],
+            modtp_recv.at[k - 1],
+            "tp",
+            lax.rem(t + k, tp),
+        )
+        copy.start()
+        mods.append(copy)
+
+    lane = lax.broadcasted_iota(jnp.int32, (WIN, 128), 1)
+    row = lax.broadcasted_iota(jnp.int32, (WIN, 128), 0)
+    quarter = HD // 4
+    inverse = jnp.exp(
+        lax.rem(lane, quarter).astype(f32) * (-jnp.log(jnp.float32(rope_base)) / quarter)
+    )
+    first = lax.rem(lane, 2 * quarter) < quarter
+
+    def tables(b, carry):
+        place = s * total + b * WIN + row
+        by_row = lax.rem(lane, HD) < HD // 2
+        coordinate = jnp.where(by_row, place // GRID_W, lax.rem(place, GRID_W))
+        angles = coordinate.astype(f32) * inverse
+        turn_cos[b] = jnp.cos(angles)
+        sines = jnp.sin(angles)
+        turn_sin[b] = jnp.where(first, -sines, sines)
+        return carry
+
+    lax.fori_loop(0, tp, tables, 0)
+
+    for copy in mods:
+        copy.wait()
+    for i in range(tp):
+        cols = slice(i * mod_cols, (i + 1) * mod_cols)
+        shift_v[:, cols] = mod_all[i, :, 0:mod_cols]
+        factor_v[:, cols] = gain_v[:, cols] * (1.0 + mod_all[i, :, mod_cols : 2 * mod_cols])
+        gate_v[:, cols] = mod_all[i, :, 2 * mod_cols : 3 * mod_cols]
+    gate_store = pltpu.make_async_copy(gate_v, gate_out, load_sem.at[len(loads)])
+    gate_store.start()
+
+    low = lane < HD
+
+    def turned(values, slot):
+        swapped = jnp.where(
+            first, pltpu.roll(values, 128 - quarter, 1), pltpu.roll(values, quarter, 1)
+        )
+        return values * turn_cos[slot] + swapped * turn_sin[slot]
+
+    def project(slot):
+        def norm_rows(g, carry):
+            part = pl.ds(pl.multiple_of(g * NORM_ROWS, NORM_ROWS), NORM_ROWS)
+            values = rows_all[slot, part].astype(f32)
+            scale = lax.rsqrt(jnp.mean(values * values, axis=-1, keepdims=True) + epsilon)
+            normed[part] = (values * scale * factor_v[...] + shift_v[...]).astype(bf16)
+            return carry
+
+        lax.fori_loop(0, rows // NORM_ROWS, norm_rows, 0)
+        base = pl.multiple_of(WIN + slot * rows, WIN)
+        prepared = normed[...]
+        q = jnp.dot(prepared, wq[...], preferred_element_type=f32)
+        k = jnp.dot(prepared, wk[...], preferred_element_type=f32)
+        v = jnp.dot(prepared, wv[...], preferred_element_type=f32)
+        key_value[pl.ds(base, rows), :key_width] = turned(k, slot).astype(bf16)
+        key_value[pl.ds(base, rows), key_width:] = v.astype(bf16)
+        factor = HD ** (-0.5)
+        for h in range(heads):
+            lanes = q[:, (h // 2) * 128 : (h // 2 + 1) * 128]
+            lanes = (turned(lanes, slot).astype(bf16).astype(f32)) * factor
+            at, want = h % 2, h // group
+            if at != want:
+                lanes = pltpu.roll(lanes, HD, 1)
+            keep = low if want == 0 else jnp.logical_not(low)
+            queries[slot, h * rows : (h + 1) * rows] = jnp.where(keep, lanes, 0.0).astype(bf16)
+
+    loads[8].wait()
+    loads[9].wait()
+
+    def fwd(j, c):
+        slot = chip_from(j) * 2 + core
+        part = pl.ds(c * piece, piece)
+        i = (j - 1) * PIECES + c
+        return remote(
+            rows_all.at[slot, part],
+            rows_all.at[slot, part],
+            fwd_send.at[i],
+            fwd_recv.at[i],
+            "tp",
+            pair,
+        )
+
+    def project_step(k, carry):
+        @pl.when(k == 1)
+        def _():
+            near.wait_recv()
+
+        for j in range(1, chips):
+
+            @pl.when(k == 2 * j)
+            def _():
+                for c in range(PIECES):
+                    far[j, c].wait_recv()
+                    fwd(j, c).start()
+
+            @pl.when(k == 2 * j + 1)
+            def _():
+                for c in range(PIECES):
+                    fwd(j, c).wait_recv()
+
+        source = lax.rem(chip + chips - k // 2, chips)
+        flip = lax.rem(k, 2)
+        project(source * 2 + core + flip - 2 * core * flip)
+        return carry
+
+    lax.fori_loop(0, tp, project_step, 0)
+
+    halo_right = remote(
+        key_value.at[pl.ds(total, WIN)],
+        key_value.at[pl.ds(0, WIN)],
+        halo_send.at[0],
+        halo_recv.at[0],
+        "sp",
+        lax.rem(s + 1, sp),
+    )
+    halo_left = remote(
+        key_value.at[pl.ds(WIN, WIN)],
+        key_value.at[pl.ds(total + WIN, WIN)],
+        halo_send.at[1],
+        halo_recv.at[1],
+        "sp",
+        lax.rem(s + sp - 1, sp),
+    )
+    halo_right.start()
+    halo_left.start()
+    for copy in ctxs:
+        copy.wait()
+    loads[10].wait()
+
+    def block_at(step):
+        return jnp.where(step < tp - 1, lax.rem(step + 1, tp - 1), tp - 1)
+
+    def att_pair(b):
+        return remote(
+            att_all.at[b, t], att_all.at[b, t], apair_send.at[b], apair_recv.at[b], "tp", pair
+        )
+
+    def att_far(b, j):
+        i = b * (chips - 1) + j - 1
+        return remote(
+            att_all.at[b, t],
+            att_all.at[b, t],
+            afar_send.at[i],
+            afar_recv.at[i],
+            "tp",
+            chip_at(j) * 2 + core,
+        )
+
+    def att_fwd(b, j):
+        slot = chip_from(j) * 2 + core
+        i = b * (chips - 1) + j - 1
+        return remote(
+            att_all.at[b, slot],
+            att_all.at[b, slot],
+            afwd_send.at[i],
+            afwd_recv.at[i],
+            "tp",
+            pair,
+        )
+
+    contract = (((1,), (1,)), ((), ()))
+    band = 3 * WIN
+    q_pos = lax.broadcasted_iota(jnp.int32, (WIN, band), 0)
+    k_pos = lax.broadcasted_iota(jnp.int32, (WIN, band), 1)
+    in_window = jnp.logical_and(k_pos >= q_pos, k_pos <= q_pos + 2 * WIN)
+
+    def attend(b):
+        start = pl.multiple_of(b * WIN, WIN)
+        band_k = key_value[pl.ds(start, band), :key_width]
+        band_v = key_value[pl.ds(start, band), key_width:]
+        ctx_k = ctx_kv[:, :, :key_width].reshape(sp * ctx_rows, key_width)
+        ctx_v_ = ctx_kv[:, :, key_width:].reshape(sp * ctx_rows, key_width)
+        place = s * total + b * WIN - WIN + k_pos
+        allowed = jnp.logical_and(
+            in_window, jnp.logical_and(place >= 0, place < sp * total)
+        )
+        results = []
+        for h in range(heads):
+            q = queries[b, h * rows : (h + 1) * rows]
+            near_s = lax.dot_general(q, band_k, contract, preferred_element_type=f32)
+            near_s = jnp.where(allowed, near_s, neg_large)
+            ctx_s = lax.dot_general(q, ctx_k, contract, preferred_element_type=f32)
+            top = jnp.maximum(
+                jnp.max(near_s, axis=-1, keepdims=True), jnp.max(ctx_s, axis=-1, keepdims=True)
+            )
+            top = jnp.maximum(top, sink[h])
+            near_e = jnp.exp(near_s - top)
+            ctx_e = jnp.exp(ctx_s - top)
+            bottom = (
+                jnp.sum(near_e, axis=-1, keepdims=True)
+                + jnp.sum(ctx_e, axis=-1, keepdims=True)
+                + jnp.exp(sink[h] - top)
+            )
+            share = 1.0 / bottom
+            results.append(
+                jnp.dot((near_e * share).astype(bf16), band_v, preferred_element_type=f32)
+                + jnp.dot((ctx_e * share).astype(bf16), ctx_v_, preferred_element_type=f32)
+            )
+        for v in range(query_width // 128):
+            sides = []
+            for at in range(2):
+                h = 2 * v + at
+                lanes = results[h]
+                if h // group != at:
+                    lanes = pltpu.roll(lanes, HD, 1)
+                sides.append(lanes)
+            att_all[b, t, :, v * 128 : (v + 1) * 128] = jnp.where(low, sides[0], sides[1]).astype(
+                bf16
+            )
+
+    def hand_on(b):
+        for j in range(1, chips):
+            att_far(b, j).wait_recv()
+            att_fwd(b, j).start()
+
+    def out_copy(b):
+        return remote(
+            out_cols.at[b],
+            blended.at[:, pl.ds(pl.multiple_of(t * out_width, 128), out_width)],
+            out_send.at[b],
+            out_recv.at[t],
+            "tp",
+            b,
+        )
+
+    own_copy = pltpu.make_async_copy(
+        out_cols.at[t],
+        blended.at[:, pl.ds(pl.multiple_of(t * out_width, 128), out_width)],
+        load_sem.at[len(loads) + 1],
+    )
+
+    def finish(b):
+        att_pair(b).wait_recv()
+        for j in range(1, chips):
+            att_fwd(b, j).wait_recv()
+        sums = jnp.dot(att_all[b, 0], wo[0:query_width], preferred_element_type=f32)
+        for i in range(1, tp):
+            sums = sums + jnp.dot(
+                att_all[b, i],
+                wo[i * query_width : (i + 1) * query_width],
+                preferred_element_type=f32,
+            )
+        out_cols[b] = sums.astype(bf16)
+
+        @pl.when(b == t)
+        def _():
+            own_copy.start()
+
+        @pl.when(b != t)
+        def _():
+            out_copy(b).start()
+
+    def attend_step(step, carry):
+        @pl.when(step < tp)
+        def _():
+            b = block_at(step)
+
+            @pl.when(step == tp - 2)
+            def _():
+                halo_right.wait_recv()
+
+            @pl.when(step == tp - 1)
+            def _():
+                halo_left.wait_recv()
+
+            attend(b)
+            att_pair(b).start()
+            for j in range(1, chips):
+                att_far(b, j).start()
+
+        @pl.when(jnp.logical_and(step >= 1, step < tp + 1))
+        def _():
+            hand_on(block_at(step - 1))
+
+        @pl.when(step >= 2)
+        def _():
+            finish(block_at(step - 2))
+
+        return carry
+
+    lax.fori_loop(0, tp + 2, attend_step, 0)
+
+    near.wait_send()
+    for copy in far.values():
+        copy.wait_send()
+    for j in range(1, chips):
+        for c in range(PIECES):
+            fwd(j, c).wait_send()
+    gate_store.wait()
+    halo_right.wait_send()
+    halo_left.wait_send()
+    for b in range(tp):
+        att_pair(b).wait_send()
+        for j in range(1, chips):
+            att_far(b, j).wait_send()
+            att_fwd(b, j).wait_send()
+    own_copy.wait()
+    for k in range(1, tp):
+        other = lax.rem(t + k, tp)
+        out_copy(other).wait_send()
+        remote(
+            out_cols.at[other],
+            blended.at[:, pl.ds(pl.multiple_of(other * out_width, 128), out_width)],
+            out_send.at[other],
+            out_recv.at[other],
+            "tp",
+            other,
+        ).wait_recv()
+
+
+def local(
+    latent,
+    context,
+    conditioning,
+    norm_gain,
+    shift_weight,
+    scale_weight,
+    gate_weight,
+    query_weight,
+    key_weight,
+    value_weight,
+    out_weight,
+    sink_logit,
+):
+    tp, sp = lax.axis_size("tp"), lax.axis_size("sp")
+    rows, width = latent.shape
+    ctx_rows = context.shape[0]
+    mod_rows, mod_cols = shift_weight.shape
+    query_width, key_width = query_weight.shape[1], key_weight.shape[1]
+    out_width = out_weight.shape[1]
+    fits = (
+        rows == WIN
+        and key_width == 2 * HD
+        and tp % 2 == 0
+        and tp >= 4
+        and sp >= 2
+        and ctx_rows % NORM_ROWS == 0
+        and mod_cols % 128 == 0
+    )
+    if not fits:
+        return local_plain(
+            latent,
+            context,
+            conditioning,
+            norm_gain,
+            shift_weight,
+            scale_weight,
+            gate_weight,
+            query_weight,
+            key_weight,
+            value_weight,
+            out_weight,
+            sink_logit,
+        )
+    f32, bf16 = jnp.float32, jnp.bfloat16
+    chips = tp // 2
+    far = (chips - 1) * PIECES
+    dma = pltpu.SemaphoreType.DMA
+    anywhere = pl.BlockSpec(memory_space=pl.ANY)
+    blended, gate = pl.pallas_call(
+        functools.partial(fused_kernel, tp, sp),
+        out_shape=(
+            jax.ShapeDtypeStruct((rows, width), bf16),
+            jax.ShapeDtypeStruct((1, width), f32),
+        ),
+        in_specs=[anywhere] * 11 + [pl.BlockSpec(memory_space=pltpu.SMEM)],
+        out_specs=(anywhere, anywhere),
+        scratch_shapes=[
+            pltpu.VMEM((1, mod_rows), bf16),
+            pltpu.VMEM((1, width), f32),
+            pltpu.VMEM((3, mod_rows, mod_cols), bf16),
+            pltpu.VMEM(query_weight.shape, bf16),
+            pltpu.VMEM(key_weight.shape, bf16),
+            pltpu.VMEM(value_weight.shape, bf16),
+            pltpu.VMEM(out_weight.shape, bf16),
+            pltpu.VMEM(context.shape, bf16),
+            pltpu.VMEM((tp, rows, width), bf16),
+            pltpu.VMEM((rows, width), bf16),
+            pltpu.VMEM((sp, 1, 3 * mod_cols), f32),
+            pltpu.VMEM((tp, 1, 3 * mod_cols), f32),
+            pltpu.VMEM((1, width), f32),
+            pltpu.VMEM((1, width), f32),
+            pltpu.VMEM((1, width), f32),
+            pltpu.VMEM((tp, rows, 128), f32),
+            pltpu.VMEM((tp, rows, 128), f32),
+            pltpu.VMEM((tp, query_width // HD * rows, key_width), bf16),
+            pltpu.VMEM(((tp + 2) * rows, 2 * key_width), bf16),
+            pltpu.VMEM((sp, ctx_rows, 2 * key_width), bf16),
+            pltpu.VMEM((tp, tp, rows, query_width), bf16),
+            pltpu.VMEM((tp, rows, out_width), bf16),
+            dma((13,)),
+            dma((1,)),
+            dma((1,)),
+            dma((far,)),
+            dma((far,)),
+            dma((far,)),
+            dma((far,)),
+            dma((sp - 1,)),
+            dma((sp - 1,)),
+            dma((tp - 1,)),
+            dma((tp - 1,)),
+            dma((sp - 1,)),
+            dma((sp - 1,)),
+            dma((2,)),
+            dma((2,)),
+            dma((tp,)),
+            dma((tp,)),
+            dma((tp * (chips - 1),)),
+            dma((tp * (chips - 1),)),
+            dma((tp * (chips - 1),)),
+            dma((tp * (chips - 1),)),
+            dma((tp,)),
+            dma((tp,)),
+        ],
+        compiler_params=pltpu.CompilerParams(
+            collective_id=0, has_side_effects=True, vmem_limit_bytes=60 * 1024 * 1024
+        ),
+        name="fused",
+    )(
+        latent,
+        context,
+        conditioning.reshape(1, mod_rows),
+        norm_gain.reshape(1, width),
+        shift_weight,
+        scale_weight,
+        gate_weight,
+        query_weight,
+        key_weight,
+        value_weight,
+        out_weight,
+        sink_logit,
+    )
+    return (latent.astype(f32) + gate * blended.astype(f32)).astype(bf16)
+
+
 def solution(mesh):
     in_specs = (
         P(("grp", "sp", "tp"), None),

time: 177 us -> 71.5 us (0.40)
  Pallas kernels: 0 us -> 67.5 us
  blocking collectives: 61.4 us -> 0 us
  matrix products: 25.8 us -> 0 us
  waiting for transfers between devices: 25.4 us -> 0 us
  local copies, waits for them, and re-layouts: 24.7 us -> 1.28 us
  between operations: 13.8 us -> 0.02 us
  other arithmetic: 13.9 us -> 2.51 us
  starting transfers between devices: 10.9 us -> 0 us
    pallas_call x0 -> x1, Pallas kernels: none -> 67.5 us  [local(): pl.pallas_call(functools.partial(fused_kernel, tp, sp), out_shape=(jax.Sh...]
    all_gather x4 -> x0, blocking collectives: 40.9 us -> none  [the longest x1 15.4 us: local(): lax.all_gather(summed[2], 'tp', axis=0, tiled=True)]
    dot_general x13 -> x0, matrix products: 25.8 us -> none  [the longest x1 4.78 us: local(): jnp.einsum('nqhgd,thd->nhgqt', query_blocks, context_keys, preferred_elem...]
    all_gather x2 -> x0, waiting for transfers between devices: 25.4 us -> none  [the longest x1 16.1 us: local(): lax.all_gather(attended, 'tp', axis=1, tiled=True)]
    psum x1 -> x0, blocking collectives: 20.5 us -> none  [local(): summed = lax.psum((shift_part, scale_part, gate_part), 'sp')]
    slice x9 -> x0, local copies, waits for them, and re-layouts: 8.46 us -> none  [the longest x1 1.72 us: local(): band_blocks[:block_count]]
    concatenate x6 -> x0, local copies, waits for them, and re-layouts: 7.93 us -> none  [the longest x5 6.19 us: axial_turn(): jnp.concatenate([turn(values[..., :half_dim], position // GRID_W), turn(v...]
    unnamed x44 -> x2, local copies, waits for them, and re-layouts: 7.79 us -> 0.01 us
  transfers between devices with their start and end apart: 5 -> 0, of which waited for: 2 -> 0; matrix products, arithmetic and copies ran while one was open for 14% -> 0% of each run, Pallas kernels for 0% -> 0%
where the time goes in v1:
time: 71.5 us; the launch traced here: 71.3 us
  Pallas kernels  67.5 us (94%)
  other arithmetic  2.51 us (4%)
  local copies, waits for them, and re-layouts  1.28 us (2%)
    pallas_call x1, Pallas kernels, local(): pl.pallas_call(functools.partial(fused_kernel, tp, sp), out_shape=(jax.Sh...  67.5 us
    convert_element_type x1, other arithmetic, local(): return (latent.astype(f32) + gate * blended.astype(f32)).astype(bf16)  2.51 us

profile of v1, /device:TPU:0, one launch (start us, length us, event | category | flops | bytes accessed | tf_op | source)
XLA Modules:
  0.0 71.3 jit_solution(13104144192879460390)
XLA Ops:
  0.0 1.3 %reshape.6.conditioning = bf16[1,1024]{1,0:T(2,128)(2,1)} reshape(bf16[1024]{0:T(1024)(128)(2,1)} %param.14) | data formatting | bytes 4096 | tf_op jit(solution)/shard_map/reshape | solution.py:839
  1.3 0.0 copy-start
  1.3 67.5 %fused.1 = (bf16[128,4096]{1,0:T(8,128)(2,1)}, f32[1,4096]{1,0:T(1,128)}) custom-call(bf16[128,4096]{1,0:T(8,128)(2,1)} %latent.1, bf16[192,4096]{1,0:T(8,128)(2,1)} %context.1, bf16[1,1024]{1,0:T(2,128)(2,1)} %reshape.6.conditioning, f32[1,4096]{1,0:T(1,128)} %bitcast.3, bf16[1024,1024]{1,0:T(8,128)(2,1)} %shift_weight.1, bf16[1024,1024]{1,0:T(8,128)(2,1)} %scale_weight.1, ...), custom_call_target="tpu_custom_call" | custom-call | tf_op jit(solution)/shard_map/fused/pallas_call | solution.py:777
  68.8 0.0 copy-done
  68.8 2.5 %add_convert_fusion = bf16[128,4096]{1,0:T(8,128)(2,1)} fusion(bf16[128,4096]{1,0:T(8,128)(2,1)} %get-tuple-element.8, bf16[128,4096]{1,0:T(8,128)(2,1)S(1)} %copy-done, f32[4096]{0:T(1024)} %bitcast.2), kind=kLoop, calls=%fused_computation | loop fusion | flops 2621440 | bytes 3162112 | tf_op jit(solution)/shard_map/convert_element_type | solution.py:850
Async XLA Ops:
  1.3 67.5 %copy-start = (bf16[128,4096]{1,0:T(8,128)(2,1)S(1)}, bf16[128,4096]{1,0:T(8,128)(2,1)}, u32[]{:S(2)}) copy-start(bf16[128,4096]{1,0:T(8,128)(2,1)} %latent.1) | copy-start | bytes 3145732

commit v2 on v1

--- a/solution.py
+++ b/solution.py
@@ -353,7 +353,7 @@
 
     for i in range(4):
         loads[i].wait()
-    cond = cond_v[...].astype(f32)
+    cond = cond_v[...].astype(f32).reshape(1, cond_v.shape[0])
     lifted = jnp.broadcast_to(cond / (1.0 + jnp.exp(-cond)), (16, cond.shape[1])).astype(bf16)
     for i in range(3):
         mod_part[s, :, i * mod_cols : (i + 1) * mod_cols] = jnp.dot(
@@ -455,31 +455,43 @@
         )
         return values * turn_cos[slot] + swapped * turn_sin[slot]
 
-    def project(slot):
+    half = rows // 2
+
+    def norm_piece(slot, first_row, count, target):
         def norm_rows(g, carry):
-            part = pl.ds(pl.multiple_of(g * NORM_ROWS, NORM_ROWS), NORM_ROWS)
-            values = rows_all[slot, part].astype(f32)
+            at = pl.multiple_of(first_row + g * NORM_ROWS, NORM_ROWS)
+            values = rows_all[slot, pl.ds(at, NORM_ROWS)].astype(f32)
             scale = lax.rsqrt(jnp.mean(values * values, axis=-1, keepdims=True) + epsilon)
-            normed[part] = (values * scale * factor_v[...] + shift_v[...]).astype(bf16)
+            normed[pl.ds(pl.multiple_of(target + at, NORM_ROWS), NORM_ROWS)] = (
+                values * scale * factor_v[...] + shift_v[...]
+            ).astype(bf16)
             return carry
 
-        lax.fori_loop(0, rows // NORM_ROWS, norm_rows, 0)
-        base = pl.multiple_of(WIN + slot * rows, WIN)
+        lax.fori_loop(0, count // NORM_ROWS, norm_rows, 0)
+
+    def project(slots):
         prepared = normed[...]
-        q = jnp.dot(prepared, wq[...], preferred_element_type=f32)
-        k = jnp.dot(prepared, wk[...], preferred_element_type=f32)
-        v = jnp.dot(prepared, wv[...], preferred_element_type=f32)
-        key_value[pl.ds(base, rows), :key_width] = turned(k, slot).astype(bf16)
-        key_value[pl.ds(base, rows), key_width:] = v.astype(bf16)
+        q_both = jnp.dot(prepared, wq[...], preferred_element_type=f32)
+        k_both = jnp.dot(prepared, wk[...], preferred_element_type=f32)
+        v_both = jnp.dot(prepared, wv[...], preferred_element_type=f32)
         factor = HD ** (-0.5)
-        for h in range(heads):
-            lanes = q[:, (h // 2) * 128 : (h // 2 + 1) * 128]
-            lanes = (turned(lanes, slot).astype(bf16).astype(f32)) * factor
-            at, want = h % 2, h // group
-            if at != want:
-                lanes = pltpu.roll(lanes, HD, 1)
-            keep = low if want == 0 else jnp.logical_not(low)
-            queries[slot, h * rows : (h + 1) * rows] = jnp.where(keep, lanes, 0.0).astype(bf16)
+        for i, slot in enumerate(slots):
+            q, k, v = (a[i * rows : (i + 1) * rows] for a in (q_both, k_both, v_both))
+            base = pl.multiple_of(WIN + slot * rows, WIN)
+            key_value[pl.ds(base, rows), :key_width] = turned(k, slot).astype(bf16)
+            key_value[pl.ds(base, rows), key_width:] = v.astype(bf16)
+            for h in range(heads):
+                lanes = q[:, (h // 2) * 128 : (h // 2 + 1) * 128]
+                lanes = (turned(lanes, slot).astype(bf16).astype(f32)) * factor
+                at, want = h % 2, h // group
+                if at != want:
+                    lanes = pltpu.roll(lanes, HD, 1)
+                keep = low if want == 0 else jnp.logical_not(low)
+                lanes = jnp.where(keep, lanes, 0.0).astype(bf16)
+                for n in range(2):
+                    queries[2 * slot + n, h * half : (h + 1) * half] = lanes[
+                        n * half : (n + 1) * half
+                    ]
 
     loads[8].wait()
     loads[9].wait()
@@ -497,30 +509,22 @@
             pair,
         )
 
-    def project_step(k, carry):
-        @pl.when(k == 1)
-        def _():
-            near.wait_recv()
-
-        for j in range(1, chips):
-
-            @pl.when(k == 2 * j)
-            def _():
-                for c in range(PIECES):
-                    far[j, c].wait_recv()
-                    fwd(j, c).start()
-
-            @pl.when(k == 2 * j + 1)
-            def _():
-                for c in range(PIECES):
-                    fwd(j, c).wait_recv()
-
-        source = lax.rem(chip + chips - k // 2, chips)
-        flip = lax.rem(k, 2)
-        project(source * 2 + core + flip - 2 * core * flip)
-        return carry
-
-    lax.fori_loop(0, tp, project_step, 0)
+    norm_piece(t, 0, rows, 0)
+    near.wait_recv()
+    norm_piece(pair, 0, rows, rows)
+    project((t, pair))
+    for j in range(1, chips):
+        mine, other = chip_from(j) * 2 + core, chip_from(j) * 2 + 1 - core
+        for c in range(PIECES):
+            far[j, c].wait_recv()
+            fwd(j, c).start()
+            norm_piece(mine, c * piece, piece, 0)
+            if c:
+                fwd(j, c - 1).wait_recv()
+                norm_piece(other, (c - 1) * piece, piece, rows)
+        fwd(j, PIECES - 1).wait_recv()
+        norm_piece(other, (PIECES - 1) * piece, piece, rows)
+        project((mine, other))
 
     halo_right = remote(
         key_value.at[pl.ds(total, WIN)],
@@ -544,8 +548,12 @@
         copy.wait()
     loads[10].wait()
 
-    def block_at(step):
-        return jnp.where(step < tp - 1, lax.rem(step + 1, tp - 1), tp - 1)
+    def halves_at(p):
+        inner = p < tp - 2
+        return (
+            jnp.where(inner, p + 2, p - (tp - 2)),
+            p + tp,
+        )
 
     def att_pair(b):
         return remote(
@@ -576,75 +584,84 @@
         )
 
     contract = (((1,), (1,)), ((), ()))
-    band = 3 * WIN
-    q_pos = lax.broadcasted_iota(jnp.int32, (WIN, band), 0)
-    k_pos = lax.broadcasted_iota(jnp.int32, (WIN, band), 1)
+    band = 2 * WIN + half
+    stack = heads * half
+    q_pos = lax.rem(lax.broadcasted_iota(jnp.int32, (stack, band), 0), half)
+    k_pos = lax.broadcasted_iota(jnp.int32, (stack, band), 1)
     in_window = jnp.logical_and(k_pos >= q_pos, k_pos <= q_pos + 2 * WIN)
-
-    def attend(b):
-        start = pl.multiple_of(b * WIN, WIN)
+    head_of = lax.broadcasted_iota(jnp.int32, (stack, 1), 0) // half
+    sinks = jnp.full((stack, 1), sink[0], f32)
+    for h in range(1, heads):
+        sinks = jnp.where(head_of == h, sink[h], sinks)
+
+    def attend(p, n, hb):
+        start = pl.multiple_of(hb * half, half)
         band_k = key_value[pl.ds(start, band), :key_width]
         band_v = key_value[pl.ds(start, band), key_width:]
         ctx_k = ctx_kv[:, :, :key_width].reshape(sp * ctx_rows, key_width)
         ctx_v_ = ctx_kv[:, :, key_width:].reshape(sp * ctx_rows, key_width)
-        place = s * total + b * WIN - WIN + k_pos
+        place = s * total + hb * half - WIN + k_pos
         allowed = jnp.logical_and(
             in_window, jnp.logical_and(place >= 0, place < sp * total)
         )
-        results = []
-        for h in range(heads):
-            q = queries[b, h * rows : (h + 1) * rows]
-            near_s = lax.dot_general(q, band_k, contract, preferred_element_type=f32)
-            near_s = jnp.where(allowed, near_s, neg_large)
-            ctx_s = lax.dot_general(q, ctx_k, contract, preferred_element_type=f32)
-            top = jnp.maximum(
-                jnp.max(near_s, axis=-1, keepdims=True), jnp.max(ctx_s, axis=-1, keepdims=True)
-            )
-            top = jnp.maximum(top, sink[h])
-            near_e = jnp.exp(near_s - top)
-            ctx_e = jnp.exp(ctx_s - top)
-            bottom = (
-                jnp.sum(near_e, axis=-1, keepdims=True)
-                + jnp.sum(ctx_e, axis=-1, keepdims=True)
-                + jnp.exp(sink[h] - top)
-            )
-            share = 1.0 / bottom
-            results.append(
-                jnp.dot((near_e * share).astype(bf16), band_v, preferred_element_type=f32)
-                + jnp.dot((ctx_e * share).astype(bf16), ctx_v_, preferred_element_type=f32)
-            )
+        q = queries[hb]
+        near_s = lax.dot_general(q, band_k, contract, preferred_element_type=f32)
+        near_s = jnp.where(allowed, near_s, neg_large)
+        ctx_s = lax.dot_general(q, ctx_k, contract, preferred_element_type=f32)
+        top = jnp.maximum(
+            jnp.max(near_s, axis=-1, keepdims=True), jnp.max(ctx_s, axis=-1, keepdims=True)
+        )
+        top = jnp.maximum(top, sinks)
+        near_e = jnp.exp(near_s - top)
+        ctx_e = jnp.exp(ctx_s - top)
+        bottom = (
+            jnp.sum(near_e, axis=-1, keepdims=True)
+            + jnp.sum(ctx_e, axis=-1, keepdims=True)
+            + jnp.exp(sinks - top)
+        )
+        share = 1.0 / bottom
+        result = jnp.dot(
+            (near_e * share).astype(bf16), band_v, preferred_element_type=f32
+        ) + jnp.dot((ctx_e * share).astype(bf16), ctx_v_, preferred_element_type=f32)
         for v in range(query_width // 128):
             sides = []
             for at in range(2):
                 h = 2 * v + at
-                lanes = results[h]
+                lanes = result[h * half : (h + 1) * half]
                 if h // group != at:
                     lanes = pltpu.roll(lanes, HD, 1)
                 sides.append(lanes)
-            att_all[b, t, :, v * 128 : (v + 1) * 128] = jnp.where(low, sides[0], sides[1]).astype(
-                bf16
-            )
+            att_all[p, t, n * half : (n + 1) * half, v * 128 : (v + 1) * 128] = jnp.where(
+                low[:half], sides[0], sides[1]
+            ).astype(bf16)
 
     def hand_on(b):
         for j in range(1, chips):
             att_far(b, j).wait_recv()
             att_fwd(b, j).start()
 
-    def out_copy(b):
+    def out_place(hb, source):
+        return blended.at[
+            pl.ds(pl.multiple_of(lax.rem(hb, 2) * half, half), half),
+            pl.ds(pl.multiple_of(source * out_width, 128), out_width),
+        ]
+
+    def out_copy(hb):
         return remote(
-            out_cols.at[b],
-            blended.at[:, pl.ds(pl.multiple_of(t * out_width, 128), out_width)],
-            out_send.at[b],
-            out_recv.at[t],
+            out_cols.at[hb],
+            out_place(hb, t),
+            out_send.at[hb],
+            out_recv.at[2 * t + lax.rem(hb, 2)],
             "tp",
-            b,
-        )
-
-    own_copy = pltpu.make_async_copy(
-        out_cols.at[t],
-        blended.at[:, pl.ds(pl.multiple_of(t * out_width, 128), out_width)],
-        load_sem.at[len(loads) + 1],
-    )
+            hb // 2,
+        )
+
+    def own_copy(hb):
+        return pltpu.make_async_copy(
+            out_cols.at[hb],
+            out_place(hb, t),
+            load_sem.at[len(loads) + 1 + lax.rem(hb, 2)],
+        )
 
     def finish(b):
         att_pair(b).wait_recv()
@@ -657,41 +674,38 @@
                 wo[i * query_width : (i + 1) * query_width],
                 preferred_element_type=f32,
             )
-        out_cols[b] = sums.astype(bf16)
-
-        @pl.when(b == t)
-        def _():
-            own_copy.start()
-
-        @pl.when(b != t)
-        def _():
-            out_copy(b).start()
+        for n, hb in enumerate(halves_at(b)):
+            out_cols[hb] = sums[n * half : (n + 1) * half].astype(bf16)
+
+            @pl.when(hb // 2 == t)
+            def _():
+                own_copy(hb).start()
+
+            @pl.when(hb // 2 != t)
+            def _():
+                out_copy(hb).start()
 
     def attend_step(step, carry):
         @pl.when(step < tp)
         def _():
-            b = block_at(step)
-
             @pl.when(step == tp - 2)
             def _():
                 halo_right.wait_recv()
-
-            @pl.when(step == tp - 1)
-            def _():
                 halo_left.wait_recv()
 
-            attend(b)
-            att_pair(b).start()
+            for n, hb in enumerate(halves_at(step)):
+                attend(step, n, hb)
             for j in range(1, chips):
-                att_far(b, j).start()
+                att_far(step, j).start()
+            att_pair(step).start()
 
         @pl.when(jnp.logical_and(step >= 1, step < tp + 1))
         def _():
-            hand_on(block_at(step - 1))
+            hand_on(step - 1)
 
         @pl.when(step >= 2)
         def _():
-            finish(block_at(step - 2))
+            finish(step - 2)
 
         return carry
 
@@ -711,18 +725,19 @@
         for j in range(1, chips):
             att_far(b, j).wait_send()
             att_fwd(b, j).wait_send()
-    own_copy.wait()
-    for k in range(1, tp):
-        other = lax.rem(t + k, tp)
-        out_copy(other).wait_send()
-        remote(
-            out_cols.at[other],
-            blended.at[:, pl.ds(pl.multiple_of(other * out_width, 128), out_width)],
-            out_send.at[other],
-            out_recv.at[other],
-            "tp",
-            other,
-        ).wait_recv()
+    for n in range(2):
+        own_copy(2 * t + n).wait()
+        for k in range(1, tp):
+            other = lax.rem(t + k, tp)
+            out_copy(2 * other + n).wait_send()
+            remote(
+                out_cols.at[2 * other + n],
+                out_place(2 * t + n, other),
+                out_send.at[2 * other + n],
+                out_recv.at[2 * other + n],
+                "tp",
+                other,
+            ).wait_recv()
 
 
 def local(
@@ -783,7 +798,7 @@
         in_specs=[anywhere] * 11 + [pl.BlockSpec(memory_space=pltpu.SMEM)],
         out_specs=(anywhere, anywhere),
         scratch_shapes=[
-            pltpu.VMEM((1, mod_rows), bf16),
+            pltpu.VMEM((mod_rows,), bf16),
             pltpu.VMEM((1, width), f32),
             pltpu.VMEM((3, mod_rows, mod_cols), bf16),
             pltpu.VMEM(query_weight.shape, bf16),
@@ -792,7 +807,7 @@
             pltpu.VMEM(out_weight.shape, bf16),
             pltpu.VMEM(context.shape, bf16),
             pltpu.VMEM((tp, rows, width), bf16),
-            pltpu.VMEM((rows, width), bf16),
+            pltpu.VMEM((2 * rows, width), bf16),
             pltpu.VMEM((sp, 1, 3 * mod_cols), f32),
             pltpu.VMEM((tp, 1, 3 * mod_cols), f32),
             pltpu.VMEM((1, width), f32),
@@ -800,12 +815,12 @@
             pltpu.VMEM((1, width), f32),
             pltpu.VMEM((tp, rows, 128), f32),
             pltpu.VMEM((tp, rows, 128), f32),
-            pltpu.VMEM((tp, query_width // HD * rows, key_width), bf16),
+            pltpu.VMEM((2 * tp, query_width // HD * (rows // 2), key_width), bf16),
             pltpu.VMEM(((tp + 2) * rows, 2 * key_width), bf16),
             pltpu.VMEM((sp, ctx_rows, 2 * key_width), bf16),
             pltpu.VMEM((tp, tp, rows, query_width), bf16),
-            pltpu.VMEM((tp, rows, out_width), bf16),
-            dma((13,)),
+            pltpu.VMEM((2 * tp, rows // 2, out_width), bf16),
+            dma((14,)),
             dma((1,)),
             dma((1,)),
             dma((far,)),
@@ -826,8 +841,8 @@
             dma((tp * (chips - 1),)),
             dma((tp * (chips - 1),)),
             dma((tp * (chips - 1),)),
-            dma((tp,)),
-            dma((tp,)),
+            dma((2 * tp,)),
+            dma((2 * tp,)),
         ],
         compiler_params=pltpu.CompilerParams(
             collective_id=0, has_side_effects=True, vmem_limit_bytes=60 * 1024 * 1024
@@ -836,7 +851,7 @@
     )(
         latent,
         context,
-        conditioning.reshape(1, mod_rows),
+        conditioning,
         norm_gain.reshape(1, width),
         shift_weight,
         scale_weight,

time: 71.5 us -> 66.7 us (0.933)
  Pallas kernels: 67.5 us -> 64 us
  local copies, waits for them, and re-layouts: 1.28 us -> 0.01 us
    pallas_call x1, Pallas kernels: 67.5 us -> 64 us  [local(): pl.pallas_call(functools.partial(fused_kernel, tp, sp), out_shape=(jax.Sh...]
    reshape x1 -> x0, local copies, waits for them, and re-layouts: 1.28 us -> none  [local(): conditioning.reshape(1, mod_rows)]
where the time goes in v2:
time: 66.7 us; the launch traced here: 66.5 us
  Pallas kernels  64 us (96%)
  other arithmetic  2.51 us (4%)
    pallas_call x1, Pallas kernels, local(): pl.pallas_call(functools.partial(fused_kernel, tp, sp), out_shape=(jax.Sh...  64 us
    convert_element_type x1, other arithmetic, local(): return (latent.astype(f32) + gate * blended.astype(f32)).astype(bf16)  2.51 us

profile of v2, /device:TPU:0, one launch (start us, length us, event | category | flops | bytes accessed | tf_op | source)
XLA Modules:
  0.0 66.5 jit_solution(15778867218094147295)
XLA Ops:
  0.0 0.0 copy-start
  0.0 64.0 %fused.1 = (bf16[128,4096]{1,0:T(8,128)(2,1)}, f32[1,4096]{1,0:T(1,128)}) custom-call(bf16[128,4096]{1,0:T(8,128)(2,1)} %latent.1, bf16[192,4096]{1,0:T(8,128)(2,1)} %context.1, bf16[1024]{0:T(1024)(128)(2,1)} %conditioning.1, f32[1,4096]{1,0:T(1,128)} %bitcast.3, bf16[1024,1024]{1,0:T(8,128)(2,1)} %shift_weight.1, bf16[1024,1024]{1,0:T(8,128)(2,1)} %scale_weight.1, ...), custom_call_target="tpu_custom_call" | custom-call | tf_op jit(solution)/shard_map/fused/pallas_call | solution.py:792
  64.0 0.0 copy-done
  64.0 2.5 %add_convert_fusion = bf16[128,4096]{1,0:T(8,128)(2,1)} fusion(bf16[128,4096]{1,0:T(8,128)(2,1)} %get-tuple-element.8, bf16[128,4096]{1,0:T(8,128)(2,1)S(1)} %copy-done, f32[4096]{0:T(1024)} %bitcast.2), kind=kLoop, calls=%fused_computation | loop fusion | flops 2621440 | bytes 3162112 | tf_op jit(solution)/shard_map/convert_element_type | solution.py:865
Async XLA Ops:
  0.0 64.0 %copy-start = (bf16[128,4096]{1,0:T(8,128)(2,1)S(1)}, bf16[128,4096]{1,0:T(8,128)(2,1)}, u32[]{:S(2)}) copy-start(bf16[128,4096]{1,0:T(8,128)(2,1)} %latent.1) | copy-start | bytes 3145732
